TPU v7x, 512 devices: a whole 4x8x8 slice. The times are simulated.
512 devices in a mesh: sp: 64 (over z, y), tp: 8 (over x, core).
Axes of the slice: x: 4, y: 8, z: 8, core: 2. Of those that a mesh axis runs over, the one named last changes fastest.
Arguments:
- resid: bfloat16 [32768, 2048], P('sp'), may hold values from -6 to 6
- queries: bfloat16 [32768, 2048], P('sp', 'tp'), may hold values from -6 to 6
- keys: bfloat16 [32768, 512], P('sp', 'tp'), may hold values from -6 to 6
- values: bfloat16 [32768, 512], P('sp', 'tp'), may hold values from -6 to 6
- documents: int32 [32768], P('sp'), may hold values from 0 to 31, never falling along the last dimension, each value on 1 to 2048 neighbouring positions
- q_gain: float32 [64], replicated, may hold values from 0.5 to 6.5
- k_gain: float32 [64], replicated, may hold values from 0.5 to 6.5
- sink: float32 [32], P('tp'), may hold values from -1 to 5
- w_out: bfloat16 [2048, 2048], P('tp'), may hold values from -0.5 to 0.5
- n_gain: float32 [2048], replicated, may hold values from 0.1 to 1.9
- w_up: bfloat16 [2048, 8192], P('sp', 'tp'), may hold values from -0.125 to 0.125
- w_down: bfloat16 [8192, 2048], P('tp', 'sp'), may hold values from -0.0625 to 0.0625
Outputs:
- layer_out: bfloat16 [32768, 2048], P('sp')
All inputs are finite; a program needn't handle non-finite values.
Results may differ from a plain program's by a relative error of at most 0.018.
The roundings to bfloat16 on the way count: a program that leaves them out, or rounds other values in their place, can miss the bound.
Values may be sent and summed in bfloat16 or wider, within the bound.
No kernel may reach another device: no remote copies, remote signals or barrier semaphores. Data moves between devices by JAX's collectives and lax.ppermute only.
A program may use at most 64 MiB of HBM per device.

v0:
```python
import jax
import jax.numpy as jnp
from jax import lax
from jax.sharding import PartitionSpec as P

WINDOW = 128


EPS = 1e-06


def gather_turned(arrays, axis, dims):
    turned = [jnp.moveaxis(a, dim, 0) for a, dim in zip(arrays, dims)]
    both = jnp.concatenate([t.reshape(len(t), -1) for t in turned], axis=1)
    result, at, outs = (lax.all_gather(both, axis, axis=0, tiled=True), 0, [])
    for t, dim in zip(turned, dims):
        section = result[:, at : at + t[0].size].reshape(-1, *t.shape[1:])
        outs.append(jnp.moveaxis(section, 0, dim))
        at += t[0].size
    return tuple(outs)


def extended(x, sides, width):
    for axis, dim in sides:
        count, length = (lax.axis_size(axis), x.shape[dim])
        up = [(i, (i + 1) % count) for i in range(count - 1)]
        down = [(j, i) for i, j in up]
        last = lax.slice_in_dim(x, length - width, length, axis=dim)
        initial = lax.slice_in_dim(x, 0, width, axis=dim)
        before = lax.ppermute(last, axis, up)
        after = lax.ppermute(initial, axis, down)
        x = jnp.concatenate([before, x, after], axis=dim)
    return x


def in_blocks(x, dim, count):
    dims = x.shape
    tiles = x.reshape(*dims[:dim], count, dims[dim] // count, *dims[dim + 1 :])
    return jnp.moveaxis(tiles, dim, 0)


def summed_on_arrival(x, axis, dim):
    count = lax.axis_size(axis)
    tiles = lax.all_to_all(in_blocks(x, dim, count), axis, 0, 0, tiled=True)
    return jnp.sum(tiles.astype(jnp.float32), axis=0)


def joined_along(tiles, dim):
    dims = list(tiles.shape[1:])
    dims[dim] *= tiles.shape[0]
    return jnp.moveaxis(tiles, 0, dim).reshape(dims)


def copy_for_each(x, axis):
    copies = jnp.broadcast_to(x, (lax.axis_size(axis), *x.shape))
    return lax.all_to_all(copies, axis, split_axis=0, concat_axis=0, tiled=True)


def collect(x, axis, dim):
    return joined_along(copy_for_each(x, axis), dim)


def rms_scale(field, gain):
    wide = field.astype(jnp.float32)
    return wide * lax.rsqrt(jnp.mean(wide * wide, axis=-1, keepdims=True) + EPS) * gain


def mixer_partial(normed, gathered):
    upward = jnp.dot(normed, gathered[0], preferred_element_type=jnp.float32)
    active = jnp.square(jax.nn.relu(upward)).astype(jnp.bfloat16)
    return jnp.dot(active, gathered[1], preferred_element_type=jnp.float32)


def shards(
    resid, queries, keys, values, documents, q_gain, k_gain, sink, w_out, n_gain, w_up, w_down
):
    rows = resid.shape[0]
    head_size = q_gain.shape[0]
    heads_here = sink.shape[0]
    kv_here = keys.shape[1] // head_size
    group = heads_here // kv_here
    gathered = None
    gathered = gather_turned((w_up, w_down), "sp", (0, 1))
    qnorm = rms_scale(queries.reshape(rows, kv_here, group, head_size), q_gain).astype(jnp.bfloat16)
    knorm = rms_scale(keys.reshape(rows, kv_here, head_size), k_gain).astype(jnp.bfloat16)
    vheads = values.reshape(rows, kv_here, head_size)
    doc_here = documents.astype(jnp.bfloat16)
    near_keys, near_values, near_docs = (
        extended(knorm, (("sp", 0),), WINDOW),
        extended(vheads, (("sp", 0),), WINDOW),
        extended(doc_here, (("sp", 0),), WINDOW),
    )
    offset = lax.axis_index("sp") * rows
    total = rows * lax.axis_size("sp")
    query_pos = offset + jnp.arange(rows, dtype=jnp.int32)
    key_pos = offset - WINDOW + jnp.arange(rows + 2 * WINDOW, dtype=jnp.int32)
    distance = key_pos[None, :] - query_pos[:, None]
    allowed = (jnp.abs(distance) <= WINDOW) & (key_pos[None, :] >= 0) & (key_pos[None, :] < total)
    allowed = allowed & (near_docs[None, :] == doc_here[:, None])
    heads_all = heads_here * lax.axis_size("tp")
    first_head = (lax.axis_index("tp") * heads_here).astype(jnp.float32)
    slopes = jnp.exp2(
        -8.0 * (first_head + jnp.arange(heads_here, dtype=jnp.float32) + 1.0) / heads_all
    )
    slopes = slopes.reshape(kv_here, group)
    sink_f = sink.reshape(kv_here, group)
    scores = jnp.einsum(
        "rkgd,skd->kgrs", qnorm, near_keys, preferred_element_type=jnp.float32
    ) * head_size ** (-0.5)
    scores = scores - slopes[:, :, None, None] * jnp.abs(distance).astype(jnp.float32)[None, None]
    scores = jnp.where(allowed[None, None], scores, jnp.float32(-1e30))
    highest = jnp.maximum(jnp.max(scores, axis=-1), sink_f[:, :, None])
    weights = jnp.exp(scores - highest[..., None])
    denom = jnp.sum(weights, axis=-1) + jnp.exp(sink_f[:, :, None] - highest)
    summed = jnp.einsum(
        "kgrs,skd->rkgd",
        weights.astype(jnp.bfloat16),
        near_values,
        preferred_element_type=jnp.float32,
    )
    attended = (
        (summed / denom.transpose(2, 0, 1)[..., None])
        .astype(jnp.bfloat16)
        .reshape(rows, heads_here * head_size)
    )
    share = rows // lax.axis_size("tp")
    head_mix = summed_on_arrival(
        jnp.dot(attended, w_out, preferred_element_type=jnp.float32).astype(jnp.bfloat16), "tp", 0
    )
    own_resid = lax.dynamic_slice_in_dim(resid, lax.axis_index("tp") * share, share, 0)
    middle = (own_resid.astype(jnp.float32) + head_mix).astype(jnp.bfloat16)
    normed_part = rms_scale(middle, n_gain).astype(jnp.bfloat16)
    normed = collect(normed_part, "tp", 0)
    partial_sum = mixer_partial(normed, gathered)
    unit_mix = summed_on_arrival(partial_sum.astype(jnp.bfloat16), "tp", 0)
    finished = (middle.astype(jnp.float32) + unit_mix).astype(jnp.bfloat16)
    return collect(finished, "tp", 0)


def solution(mesh):
    placed = (
        P("sp", None),
        P("sp", "tp"),
        P("sp", "tp"),
        P("sp", "tp"),
        P("sp"),
        P(),
        P(),
        P("tp"),
        P("tp", None),
        P(),
        P("sp", "tp"),
        P("tp", "sp"),
    )
    return jax.shard_map(
        shards, mesh=mesh, in_specs=placed, out_specs=P("sp", None), check_vma=False
    )
```

profile of v0, /device:TPU:1, one launch (start us, length us, event | category | flops | bytes accessed | tf_op | source)
XLA Modules:
  0.0 194.1 jit_solution(1907560911907022125)
XLA Ops:
  6.5 0.0 copy-start
  6.5 0.0 all-gather.2.cloned.1.call-start
  6.5 1.6 pad_maximum_fusion
  8.2 0.0 all-gather.2.cloned.1.call-update
  8.2 0.7 convert_element_type.85
  8.9 4.0 %collective-permute-start.2 = (bf16[128]{0:T(256)(128)(2,1)S(1)}, bf16[128]{0:T(256)(128)(2,1)S(1)}, u32[]{:S(2)}, u32[]{:S(2)}) collective-permute-start(bf16[128]{0:T(256)(128)(2,1)S(1)} %get-tuple-element.11), channel_id=1, source_target_pairs={{0,8},{8,16},{16,24},{24,32},{32,40},{40,48},{48,56},{56,64},{64,7... | collective-permute-start | bytes 776 | tf_op jit(solution)/shard_map/ppermute | solution.py:30
  12.9 1.3 collective-permute-start.3
  14.2 0.9 fusion.39
  15.1 0.9 fusion.41
  16.0 4.0 %collective-permute-start.4 = (bf16[128,1,64]{0,2,1:T(8,128)(2,1)S(1)}, bf16[128,1,64]{0,2,1:T(8,128)(2,1)S(1)}, u32[]{:S(2)}, u32[]{:S(2)}) collective-permute-start(bf16[128,1,64]{0,2,1:T(8,128)(2,1)S(1)} %get-tuple-element.9), channel_id=1, source_target_pairs={{0,8},{8,16},{16,24},{24,32},{32,40},{40,48},{48,56},{56,64},{64,7... | collective-permute-start | bytes 49160 | tf_op jit(solution)/shard_map/ppermute | solution.py:30
  20.0 1.3 collective-permute-start.5
  21.3 0.7 slice_bitcast_fusion.3
  22.1 4.0 %collective-permute-start = (bf16[128,1,64]{0,2,1:T(8,128)(2,1)S(1)}, bf16[128,1,64]{0,2,1:T(8,128)(2,1)S(1)}, u32[]{:S(2)}, u32[]{:S(2)}) collective-permute-start(bf16[128,1,64]{0,2,1:T(8,128)(2,1)S(1)} %get-tuple-element.7), channel_id=1, source_target_pairs={{0,8},{8,16},{16,24},{24,32},{32,40},{40,48},{48,56},{56,64},{64,7... | collective-permute-start | bytes 49160 | tf_op jit(solution)/shard_map/ppermute | solution.py:30
  26.1 1.1 copy.15
  27.2 0.1 bitcast_reduce_fusion
  27.3 0.9 fusion.67
  28.2 0.3 fusion.16
  28.6 0.7 mul.141
  29.2 0.1 mul.142
  29.3 0.1 fusion.34
  29.4 0.0 collective-permute-done.2
  29.4 1.3 collective-permute-start.1
  30.8 0.0 collective-permute-done.3
  30.8 1.0 fusion.20
  31.8 0.0 collective-permute-done.4
  31.8 0.0 collective-permute-done.5
  31.8 0.0 copy-start.3
  31.8 1.9 fusion.7
  33.7 0.0 copy-start.1
  33.7 0.0 copy-done.3
  33.7 0.1 broadcast_maximum_fusion
  33.8 1.9 fusion.1
  35.6 0.1 fusion.54
  35.7 0.0 collective-permute-done
  35.7 0.0 collective-permute-done.1
  35.7 0.0 copy-done.1
  35.8 2.3 %fusion.30 = bf16[512,1,4,64]{0,3,2,1:T(8,128)(2,1)S(1)} fusion(f32[768,512,4]{1,0,2:T(8,128)S(1)} %get-tuple-element.14, f32[4,512]{1,0:T(4,128)S(1)} %broadcast_maximum_fusion, f32[512,768]{0,1:T(8,128)S(1)} %fusion.16, f32[4]{0:T(128)S(1)} %multiply_exponential_fusion, pred[512,768]{0,1:T(8,128)(4,1)S(1)} %fusion.20, f32[512,4]{0,1:T(4,128)S(1)} %fusion.54, ...), kind=kOutput, calls=%fused_computation.26 | convolution fusion | flops 211320832 | bytes 8634384 | tf_op jit(solution)/shard_map/kgrs,skd->rkgd/dot_general | solution.py:115
  38.1 0.0 copy-done
  38.1 2.1 %convolution_convert_fusion = bf16[512,2048]{1,0:T(8,128)(2,1)} fusion(bf16[512,256]{0,1:T(8,128)(2,1)S(1)} %bitcast.93, bf16[256,2048]{1,0:T(8,128)(2,1)S(1)} %copy-done), kind=kOutput, calls=%fused_computation.15 | convolution fusion | flops 537919488 | bytes 3407872 | tf_op jit(solution)/shard_map/dot_general | solution.py:128
  40.2 0.0 copy-start.2
  40.2 8.9 %all-to-all-start = ((bf16[8,64,2048]{2,1,0:T(8,128)(2,1)}), bf16[8,64,2048]{2,1,0:T(8,128)(2,1)S(1)}, u32[]{:S(2)}, u32[]{:S(2)}) async-start(bf16[8,64,2048]{2,1,0:T(8,128)(2,1)} %bitcast.23), calls=%async_computation | async-start | bytes 4194304 | tf_op jit(solution)/shard_map/all_to_all | solution.py:44
  49.0 26.2 %all-to-all-done = bf16[8,64,2048]{2,1,0:T(8,128)(2,1)S(1)} async-done(((bf16[8,64,2048]{2,1,0:T(8,128)(2,1)}), bf16[8,64,2048]{2,1,0:T(8,128)(2,1)S(1)}, u32[]{:S(2)}, u32[]{:S(2)}) %all-to-all-start) | async-done | bytes 2097184 | tf_op jit(solution)/shard_map/all_to_all | solution.py:44
  75.3 0.4 convert_reduce_fusion.1
  75.6 1.1 fusion.35
  76.8 0.0 copy-done.2
  76.8 0.1 fusion.37
  77.0 0.2 broadcast_in_dim.14
  77.2 29.6 %all_to_all.20 = bf16[8,64,2048]{2,1,0:T(8,128)(2,1)S(1)} all-to-all(bf16[8,64,2048]{2,1,0:T(8,128)(2,1)S(1)} %broadcast_in_dim.14), channel_id=1, replica_groups=mesh['sp'=64,'tp'=8] {'tp'}, dimensions={0} | all-to-all | bytes 4194304 | tf_op jit(solution)/shard_map/all_to_all | solution.py:56
  106.8 8.1 %all-gather.2.cloned.1.call-done = bf16[2048,2048]{1,0:T(8,128)(2,1)} async-done(((bf16[32,2048]{1,0:T(8,128)(2,1)}), bf16[2048,2048]{1,0:T(8,128)(2,1)}) %all-gather.2.cloned.1.call-update) | async-done | bytes 8388624 | tf_op jit(solution)/shard_map/all_gather | solution.py:15
  115.0 9.3 %fusion.11 = bf16[512,2048]{1,0:T(8,128)(2,1)} fusion(bf16[2048,2048]{1,0:T(8,128)(2,1)} %all-gather.2.cloned.1.call-done, bf16[512,2048]{1,0:T(8,128)(2,1)S(1)} %bitcast.91), kind=kOutput, calls=%fused_computation.14 | convolution fusion | flops 4297588736 | bytes 12582912 | tf_op jit(solution)/shard_map/dot_general | solution.py:71
  124.3 31.3 %all_to_all.21 = bf16[8,64,2048]{2,1,0:T(8,128)(2,1)S(1)} all-to-all(bf16[8,64,2048]{2,1,0:T(8,128)(2,1)} %bitcast.92), channel_id=1, replica_groups=mesh['sp'=64,'tp'=8] {'tp'}, dimensions={0} | all-to-all | bytes 4194304 | tf_op jit(solution)/shard_map/all_to_all | solution.py:44
  155.6 0.4 convert_reduce_fusion
  156.0 0.1 fusion.38
  156.1 0.2 broadcast_in_dim.15
  156.3 29.7 %all_to_all.22 = bf16[8,64,2048]{2,1,0:T(8,128)(2,1)S(1)} all-to-all(bf16[8,64,2048]{2,1,0:T(8,128)(2,1)S(1)} %broadcast_in_dim.15), channel_id=1, replica_groups=mesh['sp'=64,'tp'=8] {'tp'}, dimensions={0} | all-to-all | bytes 4194304 | tf_op jit(solution)/shard_map/all_to_all | solution.py:56
  186.0 1.3 copy.19
  (10 shorter events, 0.1 us)
Async XLA Ops:
  6.5 31.6 %copy-start = (bf16[256,2048]{1,0:T(8,128)(2,1)S(1)}, bf16[256,2048]{1,0:T(8,128)(2,1)}, u32[]{:S(2)}) copy-start(bf16[256,2048]{1,0:T(8,128)(2,1)} %param.20) | copy-start | bytes 3145732
  6.5 108.4 %all-gather.2.cloned.1.call-start = ((), (), s32[]{:S(2)}) async-start(), calls=%async_computation.4 | async-start | bytes 8519680 | tf_op jit(solution)/shard_map/all_gather | solution.py:15
  8.9 20.5 %collective-permute-start.2 = (bf16[128]{0:T(256)(128)(2,1)S(1)}, bf16[128]{0:T(256)(128)(2,1)S(1)}, u32[]{:S(2)}, u32[]{:S(2)}) collective-permute-start(bf16[128]{0:T(256)(128)(2,1)S(1)} %get-tuple-element.11), channel_id=1, source_target_pairs={{0,8},{8,16},{16,24},{24,32},{32,40},{40,48},{48,56},{56,64},{64,7... | collective-permute-start | bytes 776 | tf_op jit(solution)/shard_map/ppermute | solution.py:30
  12.9 17.8 %collective-permute-start.3 = (bf16[128]{0:T(256)(128)(2,1)S(1)}, bf16[128]{0:T(256)(128)(2,1)S(1)}, u32[]{:S(2)}, u32[]{:S(2)}) collective-permute-start(bf16[128]{0:T(256)(128)(2,1)S(1)} %get-tuple-element.12), channel_id=1, source_target_pairs={{8,0},{16,8},{24,16},{32,24},{40,32},{48,40},{56,48},{64,56},{72,6... | collective-permute-start | bytes 776 | tf_op jit(solution)/shard_map/ppermute | solution.py:31
  16.0 15.7 %collective-permute-start.4 = (bf16[128,1,64]{0,2,1:T(8,128)(2,1)S(1)}, bf16[128,1,64]{0,2,1:T(8,128)(2,1)S(1)}, u32[]{:S(2)}, u32[]{:S(2)}) collective-permute-start(bf16[128,1,64]{0,2,1:T(8,128)(2,1)S(1)} %get-tuple-element.9), channel_id=1, source_target_pairs={{0,8},{8,16},{16,24},{24,32},{32,40},{40,48},{48,56},{56,64},{64,7... | collective-permute-start | bytes 49160 | tf_op jit(solution)/shard_map/ppermute | solution.py:30
  20.0 11.8 %collective-permute-start.5 = (bf16[128,1,64]{0,2,1:T(8,128)(2,1)S(1)}, bf16[128,1,64]{0,2,1:T(8,128)(2,1)S(1)}, u32[]{:S(2)}, u32[]{:S(2)}) collective-permute-start(bf16[128,1,64]{0,2,1:T(8,128)(2,1)S(1)} %get-tuple-element.10), channel_id=1, source_target_pairs={{8,0},{16,8},{24,16},{32,24},{40,32},{48,40},{56,48},{64,56},{72,6... | collective-permute-start | bytes 49160 | tf_op jit(solution)/shard_map/ppermute | solution.py:31
  22.1 13.7 %collective-permute-start = (bf16[128,1,64]{0,2,1:T(8,128)(2,1)S(1)}, bf16[128,1,64]{0,2,1:T(8,128)(2,1)S(1)}, u32[]{:S(2)}, u32[]{:S(2)}) collective-permute-start(bf16[128,1,64]{0,2,1:T(8,128)(2,1)S(1)} %get-tuple-element.7), channel_id=1, source_target_pairs={{0,8},{8,16},{16,24},{24,32},{32,40},{40,48},{48,56},{56,64},{64,7... | collective-permute-start | bytes 49160 | tf_op jit(solution)/shard_map/ppermute | solution.py:30
  29.4 6.3 %collective-permute-start.1 = (bf16[128,1,64]{0,2,1:T(8,128)(2,1)S(1)}, bf16[128,1,64]{0,2,1:T(8,128)(2,1)S(1)}, u32[]{:S(2)}, u32[]{:S(2)}) collective-permute-start(bf16[128,1,64]{0,2,1:T(8,128)(2,1)S(1)} %get-tuple-element.8), channel_id=1, source_target_pairs={{8,0},{16,8},{24,16},{32,24},{40,32},{48,40},{56,48},{64,56},{72,6... | collective-permute-start | bytes 49160 | tf_op jit(solution)/shard_map/ppermute | solution.py:31
  31.8 1.9 copy-start.3
  33.7 2.1 %copy-start.1 = (bf16[512,64]{0,1:T(8,128)(2,1)S(1)}, bf16[512,64]{0,1:T(8,128)(2,1)}, u32[]{:S(2)}) copy-start(bf16[512,64]{0,1:T(8,128)(2,1)} %param.15) | copy-start | bytes 196612
  40.2 36.6 %copy-start.2 = (f32[2048]{0:T(1024)S(1)}, f32[2048]{0:T(1024)}, u32[]{:S(2)}) copy-start(f32[2048]{0:T(1024)} %param.21) | copy-start | bytes 24580
  40.2 35.1 %all-to-all-start = ((bf16[8,64,2048]{2,1,0:T(8,128)(2,1)}), bf16[8,64,2048]{2,1,0:T(8,128)(2,1)S(1)}, u32[]{:S(2)}, u32[]{:S(2)}) async-start(bf16[8,64,2048]{2,1,0:T(8,128)(2,1)} %bitcast.23), calls=%async_computation | async-start | bytes 4194304 | tf_op jit(solution)/shard_map/all_to_all | solution.py:44
Sparse Core Ops, SparseCore 0:
  10.4 104.5 all-gather.1
where the time goes:
time: 195 us; the launch traced here: 194 us
  blocking collectives  90.6 us (46%)
  waiting for transfers between devices  34.4 us (18%)
  starting transfers between devices  24.7 us (13%)
  matrix products  15.6 us (8%)
  between operations  13.7 us (7%)
  other arithmetic  10.7 us (5%)
  local copies, waits for them, and re-layouts  4.41 us (2%)
    all_to_all x2, blocking collectives, copy_for_each(): return lax.all_to_all(copies, axis, split_axis=0, concat_axis=0, tiled=True)  59.3 us
    all_to_all x1, blocking collectives, summed_on_arrival(): tiles = lax.all_to_all(in_blocks(x, dim, count), axis, 0, 0, tiled=True)  31.3 us
    all_to_all x1, waiting for transfers between devices, summed_on_arrival(): tiles = lax.all_to_all(in_blocks(x, dim, count), axis, 0, 0, tiled=True)  26.2 us
    ppermute x3, starting transfers between devices, extended(): before = lax.ppermute(last, axis, up)  12 us
    dot_general x1, matrix products, mixer_partial(): return jnp.dot(active, gathered[1], preferred_element_type=jnp.float32)  9.31 us
    all_to_all x1, starting transfers between devices, summed_on_arrival(): tiles = lax.all_to_all(in_blocks(x, dim, count), axis, 0, 0, tiled=True)  8.88 us
    all_gather x1, waiting for transfers between devices, gather_turned(): result, at, outs = (lax.all_gather(both, axis, axis=0, tiled=True), 0, [])  8.14 us
  transfers between devices with their start and end apart: 8, of which 2 were waited for; matrix products, arithmetic and copies ran while one was open for 9% of the time, Pallas kernels for 0%

commit v1 on v0

v1 whole, which is shorter than its diff:
```python
import jax
import jax.numpy as jnp
from jax import lax
from jax.sharding import Mesh
from jax.sharding import PartitionSpec as P

WINDOW = 128
EPS = 1e-06
SP = ("z", "y")
TP = ("x", "c")


def shift(x, axis, by):
    n = lax.axis_size(axis)
    return lax.ppermute(x, axis, [(i, (i + by) % n) for i in range(n)])


def swap(x):
    return lax.ppermute(x, "c", [(0, 1), (1, 0)])


def extended(x, width):
    count, length = lax.axis_size("z") * lax.axis_size("y"), x.shape[0]
    up = [(i, (i + 1) % count) for i in range(count - 1)]
    down = [(j, i) for i, j in up]
    before = lax.ppermute(x[length - width :], SP, up)
    after = lax.ppermute(x[:width], SP, down)
    return jnp.concatenate([before, x, after], axis=0)


def rms_scale(field, gain):
    wide = field.astype(jnp.float32)
    return wide * lax.rsqrt(jnp.mean(wide * wide, axis=-1, keepdims=True) + EPS) * gain


def scatter_x(x):
    n = lax.axis_size("x")
    tiles = lax.all_to_all(x.reshape(n, x.shape[0] // n, x.shape[1]), "x", 0, 0, tiled=True)
    return jnp.sum(tiles.astype(jnp.float32), axis=0)


def gather_x(x):
    n = lax.axis_size("x")
    tiles = lax.all_to_all(jnp.broadcast_to(x, (n, *x.shape)), "x", 0, 0, tiled=True)
    return tiles.reshape(n * x.shape[0], x.shape[1])


def mixer(normed, up, down_t):
    upward = jnp.dot(normed, up, preferred_element_type=jnp.float32)
    active = jnp.square(jax.nn.relu(upward)).astype(jnp.bfloat16)
    return lax.dot_general(
        active, down_t, (((1,), (1,)), ((), ())), preferred_element_type=jnp.float32
    )


def shards(
    resid, queries, keys, values, documents, q_gain, k_gain, sink, w_out, n_gain, w_up, w_down
):
    rows = resid.shape[0]
    head_size = q_gain.shape[0]
    heads_here = sink.shape[0]
    kv_here = keys.shape[1] // head_size
    group = heads_here // kv_here
    core = lax.axis_index("c")
    units = w_up.shape[1]
    both = lax.all_gather(jnp.concatenate([w_up, w_down.T], axis=1), SP, axis=0, tiled=True)
    w_out_other = swap(w_out)
    qnorm = rms_scale(queries.reshape(rows, kv_here, group, head_size), q_gain).astype(jnp.bfloat16)
    knorm = rms_scale(keys.reshape(rows, kv_here, head_size), k_gain).astype(jnp.bfloat16)
    vheads = values.reshape(rows, kv_here, head_size)
    doc_here = documents.astype(jnp.bfloat16)
    near_keys = extended(knorm, WINDOW)
    near_values = extended(vheads, WINDOW)
    near_docs = extended(doc_here, WINDOW)
    offset = lax.axis_index(SP) * rows
    total = rows * lax.axis_size(SP)
    query_pos = offset + jnp.arange(rows, dtype=jnp.int32)
    key_pos = offset - WINDOW + jnp.arange(rows + 2 * WINDOW, dtype=jnp.int32)
    distance = key_pos[None, :] - query_pos[:, None]
    allowed = (jnp.abs(distance) <= WINDOW) & (key_pos[None, :] >= 0) & (key_pos[None, :] < total)
    allowed = allowed & (near_docs[None, :] == doc_here[:, None])
    heads_all = heads_here * lax.axis_size(TP)
    first_head = (lax.axis_index(TP) * heads_here).astype(jnp.float32)
    slopes = jnp.exp2(
        -8.0 * (first_head + jnp.arange(heads_here, dtype=jnp.float32) + 1.0) / heads_all
    )
    slopes = slopes.reshape(kv_here, group)
    sink_f = sink.reshape(kv_here, group)
    scores = jnp.einsum(
        "rkgd,skd->kgrs", qnorm, near_keys, preferred_element_type=jnp.float32
    ) * head_size ** (-0.5)
    scores = scores - slopes[:, :, None, None] * jnp.abs(distance).astype(jnp.float32)[None, None]
    scores = jnp.where(allowed[None, None], scores, jnp.float32(-1e30))
    highest = jnp.maximum(jnp.max(scores, axis=-1), sink_f[:, :, None])
    weights = jnp.exp(scores - highest[..., None])
    denom = jnp.sum(weights, axis=-1) + jnp.exp(sink_f[:, :, None] - highest)
    summed = jnp.einsum(
        "kgrs,skd->rkgd",
        weights.astype(jnp.bfloat16),
        near_values,
        preferred_element_type=jnp.float32,
    )
    attended = (
        (summed / denom.transpose(2, 0, 1)[..., None])
        .astype(jnp.bfloat16)
        .reshape(rows, heads_here * head_size)
    )
    half = rows // 2
    share = rows // lax.axis_size(TP)
    att_own = lax.dynamic_slice_in_dim(attended, core * half, half, 0)
    att_other = swap(lax.dynamic_slice_in_dim(attended, (1 - core) * half, half, 0))
    partial = jnp.dot(att_own, w_out, preferred_element_type=jnp.float32) + jnp.dot(
        att_other, w_out_other, preferred_element_type=jnp.float32
    )
    head_mix = scatter_x(partial.astype(jnp.bfloat16))
    start = core * half + lax.axis_index("x") * share
    own_resid = lax.dynamic_slice_in_dim(resid, start, share, 0)
    middle = (own_resid.astype(jnp.float32) + head_mix).astype(jnp.bfloat16)
    normed = gather_x(rms_scale(middle, n_gain).astype(jnp.bfloat16))
    normed_other = swap(normed)
    up, down_t = both[:, :units], both[:, units:]
    sent = swap(mixer(normed_other, up, down_t).astype(jnp.bfloat16))
    partial_sum = mixer(normed, up, down_t) + sent.astype(jnp.float32)
    unit_mix = scatter_x(partial_sum.astype(jnp.bfloat16))
    finished = gather_x((middle.astype(jnp.float32) + unit_mix).astype(jnp.bfloat16))
    finished_other = swap(finished)
    low = jnp.where(core == 0, finished, finished_other)
    high = jnp.where(core == 0, finished_other, finished)
    return jnp.concatenate([low, high], axis=0)


def solution(mesh):
    fine = Mesh(mesh.devices.reshape(8, 8, 4, 2), ("z", "y", "x", "c"))
    placed = (
        P(SP, None),
        P(SP, TP),
        P(SP, TP),
        P(SP, TP),
        P(SP),
        P(),
        P(),
        P(TP),
        P(TP, None),
        P(),
        P(SP, TP),
        P(TP, SP),
    )
    return jax.shard_map(
        shards, mesh=fine, in_specs=placed, out_specs=P(SP, None), check_vma=False
    )
```

time: 195 us -> 183 us (0.938)
  blocking collectives: 90.6 us -> 51.7 us
  starting transfers between devices: 24.7 us -> 39.1 us
  waiting for transfers between devices: 34.4 us -> 42.4 us
  matrix products: 15.6 us -> 18.9 us
  other arithmetic: 10.7 us -> 13.5 us
    all_to_all x3, blocking collectives: 90.6 us -> 51.7 us  [the longest x2 33.1 us: gather_x(): lax.all_to_all(jnp.broadcast_to(x, (n, *x.shape)), 'x', 0, 0, tiled=True)]
    ppermute x6 -> x11, starting transfers between devices: 15.8 us -> 35.6 us  [the longest x5 19.7 us: swap(): return lax.ppermute(x, 'c', [(0, 1), (1, 0)])]
    all_gather x1, waiting for transfers between devices: 8.14 us -> 22.1 us  [shards(): lax.all_gather(jnp.concatenate([w_up, w_down.T], axis=1), SP, axis=0, til...]
    all_to_all x1, waiting for transfers between devices: 26.2 us -> 15 us  [scatter_x(): lax.all_to_all(x.reshape(n, x.shape[0] // n, x.shape[1]), 'x', 0, 0, tile...]
    all_to_all x1, starting transfers between devices: 8.88 us -> 3.52 us  [scatter_x(): lax.all_to_all(x.reshape(n, x.shape[0] // n, x.shape[1]), 'x', 0, 0, tile...]
    ppermute x6 -> x11, waiting for transfers between devices: 0.02 us -> 5.36 us  [the longest x5 5.34 us: swap(): return lax.ppermute(x, 'c', [(0, 1), (1, 0)])]
    dot_general x2 -> x4, matrix products: 11.4 us -> 14.5 us  [the longest x2 12.6 us: mixer(): lax.dot_general(active, down_t, (((1,), (1,)), ((), ())), preferred_eleme...]
  transfers between devices with their start and end apart: 8 -> 13, of which waited for: 2 -> 5; matrix products, arithmetic and copies ran while one was open for 9% -> 13% of each run, Pallas kernels for 0% -> 0%
where the time goes in v1:
time: 183 us; the launch traced here: 182 us
  blocking collectives  51.7 us (28%)
  waiting for transfers between devices  42.4 us (23%)
  starting transfers between devices  39.1 us (21%)
  matrix products  18.9 us (10%)
  between operations  13.8 us (8%)
  other arithmetic  13.5 us (7%)
  local copies, waits for them, and re-layouts  2.85 us (2%)
    all_to_all x2, blocking collectives, gather_x(): lax.all_to_all(jnp.broadcast_to(x, (n, *x.shape)), 'x', 0, 0, tiled=True)  33.1 us
    all_gather x1, waiting for transfers between devices, shards(): lax.all_gather(jnp.concatenate([w_up, w_down.T], axis=1), SP, axis=0, til...  22.1 us
    ppermute x5, starting transfers between devices, swap(): return lax.ppermute(x, 'c', [(0, 1), (1, 0)])  19.7 us
    all_to_all x1, blocking collectives, scatter_x(): lax.all_to_all(x.reshape(n, x.shape[0] // n, x.shape[1]), 'x', 0, 0, tile...  18.7 us
    all_to_all x1, waiting for transfers between devices, scatter_x(): lax.all_to_all(x.reshape(n, x.shape[0] // n, x.shape[1]), 'x', 0, 0, tile...  15 us
    dot_general x2, matrix products, mixer(): lax.dot_general(active, down_t, (((1,), (1,)), ((), ())), preferred_eleme...  12.6 us
    ppermute x3, starting transfers between devices, extended(): before = lax.ppermute(x[length - width:], SP, up)  12 us
    ppermute x5, waiting for transfers between devices, swap(): return lax.ppermute(x, 'c', [(0, 1), (1, 0)])  5.34 us
  transfers between devices with their start and end apart: 13, of which 5 were waited for; matrix products, arithmetic and copies ran while one was open for 13% of the time, Pallas kernels for 0%

profile of v1, /device:TPU:1, one launch (start us, length us, event | category | flops | bytes accessed | tf_op | source)
XLA Modules:
  0.0 182.3 jit_solution(13644735509685345208)
XLA Ops:
  6.5 1.5 pad_maximum_fusion.1
  8.1 0.0 all-gather.2.cloned.1.call-update
  8.1 0.7 convert_element_type.94
  8.8 4.0 %collective-permute-start.2 = (bf16[128]{0:T(256)(128)(2,1)S(1)}, bf16[128]{0:T(256)(128)(2,1)S(1)}, u32[]{:S(2)}, u32[]{:S(2)}) collective-permute-start(bf16[128]{0:T(256)(128)(2,1)S(1)} %get-tuple-element.13), channel_id=1, source_target_pairs={{0,8},{8,16},{16,24},{24,32},{32,40},{40,48},{48,56},{56,64},{64,7... | collective-permute-start | bytes 776 | tf_op jit(solution)/shard_map/ppermute | solution.py:26
  12.8 1.3 collective-permute-start.3
  14.1 0.9 fusion.63
  15.0 0.9 fusion.65
  15.9 4.0 %collective-permute-start.4 = (bf16[128,1,64]{0,2,1:T(8,128)(2,1)S(1)}, bf16[128,1,64]{0,2,1:T(8,128)(2,1)S(1)}, u32[]{:S(2)}, u32[]{:S(2)}) collective-permute-start(bf16[128,1,64]{0,2,1:T(8,128)(2,1)S(1)} %get-tuple-element.11), channel_id=1, source_target_pairs={{0,8},{8,16},{16,24},{24,32},{32,40},{40,48},{48,56},{56,64},{64,7... | collective-permute-start | bytes 49160 | tf_op jit(solution)/shard_map/ppermute | solution.py:26
  19.9 1.3 collective-permute-start.5
  21.2 0.7 slice_bitcast_fusion.3
  22.0 4.0 %collective-permute-start = (bf16[128,1,64]{0,2,1:T(8,128)(2,1)S(1)}, bf16[128,1,64]{0,2,1:T(8,128)(2,1)S(1)}, u32[]{:S(2)}, u32[]{:S(2)}) collective-permute-start(bf16[128,1,64]{0,2,1:T(8,128)(2,1)S(1)} %get-tuple-element.9), channel_id=1, source_target_pairs={{0,8},{8,16},{16,24},{24,32},{32,40},{40,48},{48,56},{56,64},{64,7... | collective-permute-start | bytes 49160 | tf_op jit(solution)/shard_map/ppermute | solution.py:26
  26.0 1.1 copy.15
  27.1 0.1 bitcast_reduce_fusion
  27.2 0.9 fusion.97
  28.2 0.3 fusion.19
  28.5 0.7 mul.156
  29.1 0.1 mul.157
  29.2 0.1 fusion.56
  29.3 0.0 collective-permute-done.2
  29.3 1.3 collective-permute-start.1
  30.6 0.0 collective-permute-done.3
  30.7 7.1 %collective-permute-start.7 = (bf16[256,2048]{1,0:T(8,128)(2,1)}, bf16[256,2048]{1,0:T(8,128)(2,1)S(1)}, u32[]{:S(2)}, u32[]{:S(2)}) collective-permute-start(bf16[256,2048]{1,0:T(8,128)(2,1)} %param.20), channel_id=1, source_target_pairs={{0,1},{1,0},{2,3},{3,2},{4,5},{5,4},{6,7},{7,6},{8,9},{9,8},{10,11... | collective-permute-start | bytes 3145736 | tf_op jit(solution)/shard_map/ppermute | solution.py:19
  37.8 1.0 fusion.23
  38.8 0.0 collective-permute-done.4
  38.8 0.0 collective-permute-done.5
  38.8 0.0 copy-start.3
  38.9 1.9 %fusion.11 = (f32[4,512]{1,0:T(4,128)S(1)}, f32[768,512,4]{1,0,2:T(8,128)S(1)}) fusion(f32[512,768]{0,1:T(8,128)S(1)} %fusion.19, f32[4]{0:T(128)S(1)} %multiply_exponential_fusion, pred[512,768]{0,1:T(8,128)(4,1)S(1)} %fusion.23, bf16[512,4,64]{0,2,1:T(8,128)(2,1)S(1)} %bitcast.100, bf16[128,1,64]{0,2,1:T(8,128)(2,1)S(1)} %collective-permute-done.5, ...), kind=kOutput, calls=%fused_computation.13 | convolution fusion | flops 209483776 | bytes 8626192 | tf_op jit(solution)/shard_map/rkgd,skd->kgrs/dot_general | solution.py:89
  40.8 0.0 copy-start.1
  40.8 0.1 broadcast_maximum_fusion
  40.9 1.9 %fusion.1 = f32[4,512]{1,0:T(4,128)S(1)} fusion(f32[768,512,4]{1,0,2:T(8,128)S(1)} %get-tuple-element.16, f32[4,512]{1,0:T(4,128)S(1)} %broadcast_maximum_fusion, f32[512,768]{0,1:T(8,128)S(1)} %fusion.19, f32[4]{0:T(128)S(1)} %multiply_exponential_fusion, pred[512,768]{0,1:T(8,128)(4,1)S(1)} %fusion.23), kind=kLoop, calls=%fused_computation.3 | loop fusion | flops 9435136 | bytes 8273936 | tf_op jit(solution)/shard_map/reduce_sum | solution.py:96
  42.8 0.1 fusion.80
  42.9 0.0 collective-permute-done
  42.9 0.0 collective-permute-done.1
  42.9 0.0 copy-start
  42.9 2.4 %fusion.52 = bf16[512,1,4,64]{0,3,2,1:T(8,128)(2,1)S(1)} fusion(f32[768,512,4]{1,0,2:T(8,128)S(1)} %get-tuple-element.16, f32[4,512]{1,0:T(4,128)S(1)} %broadcast_maximum_fusion, f32[512,768]{0,1:T(8,128)S(1)} %fusion.19, f32[4]{0:T(128)S(1)} %multiply_exponential_fusion, pred[512,768]{0,1:T(8,128)(4,1)S(1)} %fusion.23, f32[512,4]{0,1:T(4,128)S(1)} %fusion.80, ...), kind=kOutput, calls=%fused_computation.39 | convolution fusion | flops 211320832 | bytes 8634384 | tf_op jit(solution)/shard_map/kgrs,skd->rkgd/dot_general | solution.py:97
  45.4 1.9 %collective-permute-start.6 = (bf16[256,256]{0,1:T(8,128)(2,1)S(1)}, bf16[256,256]{0,1:T(8,128)(2,1)S(1)}, u32[]{:S(2)}, u32[]{:S(2)}) collective-permute-start(bf16[256,256]{0,1:T(8,128)(2,1)S(1)} %constant_dynamic-slice_fusion), channel_id=1, source_target_pairs={{0,1},{1,0},{2,3},{3,2},{4,5},{5,4},{6,7},{7,6},{8,9},{9,8},{10,11... | collective-permute-start | bytes 393224 | tf_op jit(solution)/shard_map/ppermute | solution.py:19
  47.3 0.5 fusion.66
  47.8 0.0 copy-start.2
  47.8 0.8 collective-permute-done.6
  48.6 0.0 collective-permute-done.7
  48.6 1.4 fusion.15
  50.0 3.5 %all-to-all-start = ((bf16[4,64,2048]{2,1,0:T(8,128)(2,1)}), bf16[4,64,2048]{2,1,0:T(8,128)(2,1)S(1)}, u32[]{:S(2)}, u32[]{:S(2)}) async-start(bf16[4,64,2048]{2,1,0:T(8,128)(2,1)} %bitcast.23), calls=%async_computation | async-start | bytes 2097152 | tf_op jit(solution)/shard_map/all_to_all | solution.py:38
  53.6 15.0 %all-to-all-done = bf16[4,64,2048]{2,1,0:T(8,128)(2,1)S(1)} async-done(((bf16[4,64,2048]{2,1,0:T(8,128)(2,1)}), bf16[4,64,2048]{2,1,0:T(8,128)(2,1)S(1)}, u32[]{:S(2)}, u32[]{:S(2)}) %all-to-all-start) | async-done | bytes 1048608 | tf_op jit(solution)/shard_map/all_to_all | solution.py:38
  68.6 0.2 convert_reduce_fusion.1
  68.7 1.1 fusion.57
  69.9 0.1 fusion.59
  70.0 0.1 broadcast_in_dim.14
  70.2 16.6 %all_to_all.20 = bf16[4,64,2048]{2,1,0:T(8,128)(2,1)S(1)} all-to-all(bf16[4,64,2048]{2,1,0:T(8,128)(2,1)S(1)} %broadcast_in_dim.14), channel_id=1, replica_groups=mesh['z'=8,'y'=8,'x'=4,'c'=2] {'x'}, dimensions={0} | all-to-all | bytes 2097152 | tf_op jit(solution)/shard_map/all_to_all | solution.py:44
  86.8 3.8 %collective-permute-start.8 = (bf16[256,2048]{1,0:T(8,128)(2,1)S(1)}, bf16[256,2048]{1,0:T(8,128)(2,1)S(1)}, u32[]{:S(2)}, u32[]{:S(2)}) collective-permute-start(bf16[256,2048]{1,0:T(8,128)(2,1)S(1)} %bitcast.96), channel_id=1, source_target_pairs={{0,1},{1,0},{2,3},{3,2},{4,5},{5,4},{6,7},{7,6},{8,9},{9,8},{10,11... | collective-permute-start | bytes 3145736 | tf_op jit(solution)/shard_map/ppermute | solution.py:19
  90.5 2.3 %collective-permute-done.8 = bf16[256,2048]{1,0:T(8,128)(2,1)S(1)} collective-permute-done((bf16[256,2048]{1,0:T(8,128)(2,1)S(1)}, bf16[256,2048]{1,0:T(8,128)(2,1)S(1)}, u32[]{:S(2)}, u32[]{:S(2)}) %collective-permute-start.8) | collective-permute-done | bytes 1048608 | tf_op jit(solution)/shard_map/ppermute | solution.py:19
  92.8 22.1 %all-gather.2.cloned.1.call-done = bf16[2048,2048]{1,0:T(8,128)(2,1)} async-done(((bf16[32,2048]{1,0:T(8,128)(2,1)}), bf16[2048,2048]{1,0:T(8,128)(2,1)}) %all-gather.2.cloned.1.call-update) | async-done | bytes 8388624 | tf_op jit(solution)/shard_map/all_gather | solution.py:66
  114.9 6.8 %fusion.16 = bf16[256,2048]{1,0:T(8,128)(2,1)} fusion(bf16[2048,2048]{1,0:T(8,128)(2,1)} %all-gather.2.cloned.1.call-done, bf16[256,2048]{1,0:T(8,128)(2,1)S(1)} %collective-permute-done.8), kind=kOutput, calls=%fused_computation.18 | convolution fusion | flops 2148794368 | bytes 10485760 | tf_op jit(solution)/shard_map/dot_general | solution.py:51
  121.6 3.0 %collective-permute-start.9 = (bf16[256,2048]{1,0:T(8,128)(2,1)}, bf16[256,2048]{1,0:T(8,128)(2,1)}, u32[]{:S(2)}, u32[]{:S(2)}) collective-permute-start(bf16[256,2048]{1,0:T(8,128)(2,1)} %fusion.16), channel_id=1, source_target_pairs={{0,1},{1,0},{2,3},{3,2},{4,5},{5,4},{6,7},{7,6},{8,9},{9,8},{10,11... | collective-permute-start | bytes 3145736 | tf_op jit(solution)/shard_map/ppermute | solution.py:19
  124.7 5.8 %fusion.5 = f32[256,2048]{1,0:T(8,128)S(1)} fusion(bf16[2048,2048]{1,0:T(8,128)(2,1)} %all-gather.2.cloned.1.call-done, bf16[256,2048]{1,0:T(8,128)(2,1)S(1)} %bitcast.97), kind=kOutput, calls=%fused_computation.7 | convolution fusion | flops 2148270080 | bytes 11534336 | tf_op jit(solution)/shard_map/dot_general | solution.py:51
  130.5 0.0 collective-permute-done.9
  130.5 1.5 add_convert_fusion
  132.0 18.7 %all_to_all.21 = bf16[4,64,2048]{2,1,0:T(8,128)(2,1)S(1)} all-to-all(bf16[4,64,2048]{2,1,0:T(8,128)(2,1)S(1)} %bitcast.95), channel_id=1, replica_groups=mesh['z'=8,'y'=8,'x'=4,'c'=2] {'x'}, dimensions={0} | all-to-all | bytes 2097152 | tf_op jit(solution)/shard_map/all_to_all | solution.py:38
  150.7 0.2 convert_reduce_fusion
  150.9 0.1 broadcast_in_dim.15
  151.0 16.5 %all_to_all.22 = bf16[4,64,2048]{2,1,0:T(8,128)(2,1)S(1)} all-to-all(bf16[4,64,2048]{2,1,0:T(8,128)(2,1)S(1)} %broadcast_in_dim.15), channel_id=1, replica_groups=mesh['z'=8,'y'=8,'x'=4,'c'=2] {'x'}, dimensions={0} | all-to-all | bytes 2097152 | tf_op jit(solution)/shard_map/all_to_all | solution.py:44
  167.5 3.9 %collective-permute-start.10 = (bf16[256,2048]{1,0:T(8,128)(2,1)S(1)}, bf16[256,2048]{1,0:T(8,128)(2,1)S(1)}, u32[]{:S(2)}, u32[]{:S(2)}) collective-permute-start(bf16[256,2048]{1,0:T(8,128)(2,1)S(1)} %bitcast.94), channel_id=1, source_target_pairs={{0,1},{1,0},{2,3},{3,2},{4,5},{5,4},{6,7},{7,6},{8,9},{9,8},{10,11... | collective-permute-start | bytes 3145736 | tf_op jit(solution)/shard_map/ppermute | solution.py:19
  171.4 2.3 %collective-permute-done.10 = bf16[256,2048]{1,0:T(8,128)(2,1)S(1)} collective-permute-done((bf16[256,2048]{1,0:T(8,128)(2,1)S(1)}, bf16[256,2048]{1,0:T(8,128)(2,1)S(1)}, u32[]{:S(2)}, u32[]{:S(2)}) %collective-permute-start.10) | collective-permute-done | bytes 1048608 | tf_op jit(solution)/shard_map/ppermute | solution.py:19
  173.6 0.2 broadcast_select_fusion.1
  173.8 1.6 pad_maximum_fusion
  (17 shorter events, 0.2 us)
Async XLA Ops:
  6.5 108.3 %all-gather.2.cloned.1.call-start = ((), (), s32[]{:S(2)}) async-start(), calls=%async_computation.4 | async-start | bytes 8519680 | tf_op jit(solution)/shard_map/all_gather | solution.py:66
  8.8 20.6 %collective-permute-start.2 = (bf16[128]{0:T(256)(128)(2,1)S(1)}, bf16[128]{0:T(256)(128)(2,1)S(1)}, u32[]{:S(2)}, u32[]{:S(2)}) collective-permute-start(bf16[128]{0:T(256)(128)(2,1)S(1)} %get-tuple-element.13), channel_id=1, source_target_pairs={{0,8},{8,16},{16,24},{24,32},{32,40},{40,48},{48,56},{56,64},{64,7... | collective-permute-start | bytes 776 | tf_op jit(solution)/shard_map/ppermute | solution.py:26
  12.8 17.9 %collective-permute-start.3 = (bf16[128]{0:T(256)(128)(2,1)S(1)}, bf16[128]{0:T(256)(128)(2,1)S(1)}, u32[]{:S(2)}, u32[]{:S(2)}) collective-permute-start(bf16[128]{0:T(256)(128)(2,1)S(1)} %get-tuple-element.14), channel_id=1, source_target_pairs={{8,0},{16,8},{24,16},{32,24},{40,32},{48,40},{56,48},{64,56},{72,6... | collective-permute-start | bytes 776 | tf_op jit(solution)/shard_map/ppermute | solution.py:27
  15.9 22.9 %collective-permute-start.4 = (bf16[128,1,64]{0,2,1:T(8,128)(2,1)S(1)}, bf16[128,1,64]{0,2,1:T(8,128)(2,1)S(1)}, u32[]{:S(2)}, u32[]{:S(2)}) collective-permute-start(bf16[128,1,64]{0,2,1:T(8,128)(2,1)S(1)} %get-tuple-element.11), channel_id=1, source_target_pairs={{0,8},{8,16},{16,24},{24,32},{32,40},{40,48},{48,56},{56,64},{64,7... | collective-permute-start | bytes 49160 | tf_op jit(solution)/shard_map/ppermute | solution.py:26
  19.9 18.9 %collective-permute-start.5 = (bf16[128,1,64]{0,2,1:T(8,128)(2,1)S(1)}, bf16[128,1,64]{0,2,1:T(8,128)(2,1)S(1)}, u32[]{:S(2)}, u32[]{:S(2)}) collective-permute-start(bf16[128,1,64]{0,2,1:T(8,128)(2,1)S(1)} %get-tuple-element.12), channel_id=1, source_target_pairs={{8,0},{16,8},{24,16},{32,24},{40,32},{48,40},{56,48},{64,56},{72,6... | collective-permute-start | bytes 49160 | tf_op jit(solution)/shard_map/ppermute | solution.py:27
  22.0 20.9 %collective-permute-start = (bf16[128,1,64]{0,2,1:T(8,128)(2,1)S(1)}, bf16[128,1,64]{0,2,1:T(8,128)(2,1)S(1)}, u32[]{:S(2)}, u32[]{:S(2)}) collective-permute-start(bf16[128,1,64]{0,2,1:T(8,128)(2,1)S(1)} %get-tuple-element.9), channel_id=1, source_target_pairs={{0,8},{8,16},{16,24},{24,32},{32,40},{40,48},{48,56},{56,64},{64,7... | collective-permute-start | bytes 49160 | tf_op jit(solution)/shard_map/ppermute | solution.py:26
  29.3 13.5 %collective-permute-start.1 = (bf16[128,1,64]{0,2,1:T(8,128)(2,1)S(1)}, bf16[128,1,64]{0,2,1:T(8,128)(2,1)S(1)}, u32[]{:S(2)}, u32[]{:S(2)}) collective-permute-start(bf16[128,1,64]{0,2,1:T(8,128)(2,1)S(1)} %get-tuple-element.10), channel_id=1, source_target_pairs={{8,0},{16,8},{24,16},{32,24},{40,32},{48,40},{56,48},{64,56},{72,6... | collective-permute-start | bytes 49160 | tf_op jit(solution)/shard_map/ppermute | solution.py:27
  30.7 18.0 %collective-permute-start.7 = (bf16[256,2048]{1,0:T(8,128)(2,1)}, bf16[256,2048]{1,0:T(8,128)(2,1)S(1)}, u32[]{:S(2)}, u32[]{:S(2)}) collective-permute-start(bf16[256,2048]{1,0:T(8,128)(2,1)} %param.20), channel_id=1, source_target_pairs={{0,1},{1,0},{2,3},{3,2},{4,5},{5,4},{6,7},{7,6},{8,9},{9,8},{10,11... | collective-permute-start | bytes 3145736 | tf_op jit(solution)/shard_map/ppermute | solution.py:19
  38.8 2.0 %copy-start.3 = (f32[4]{0:T(128)S(1)}, f32[4]{0:T(128)}, u32[]{:S(2)}) copy-start(f32[4]{0:T(128)} %param.19) | copy-start | bytes 52
  40.8 2.1 %copy-start.1 = (bf16[512,64]{0,1:T(8,128)(2,1)S(1)}, bf16[512,64]{0,1:T(8,128)(2,1)}, u32[]{:S(2)}) copy-start(bf16[512,64]{0,1:T(8,128)(2,1)} %param.15) | copy-start | bytes 196612
  42.9 4.4 %copy-start = (bf16[256,2048]{1,0:T(8,128)(2,1)S(1)}, bf16[256,2048]{1,0:T(8,128)(2,1)}, u32[]{:S(2)}) copy-start(bf16[256,2048]{1,0:T(8,128)(2,1)} %param.20) | copy-start | bytes 3145732
  45.4 3.2 %collective-permute-start.6 = (bf16[256,256]{0,1:T(8,128)(2,1)S(1)}, bf16[256,256]{0,1:T(8,128)(2,1)S(1)}, u32[]{:S(2)}, u32[]{:S(2)}) collective-permute-start(bf16[256,256]{0,1:T(8,128)(2,1)S(1)} %constant_dynamic-slice_fusion), channel_id=1, source_target_pairs={{0,1},{1,0},{2,3},{3,2},{4,5},{5,4},{6,7},{7,6},{8,9},{9,8},{10,11... | collective-permute-start | bytes 393224 | tf_op jit(solution)/shard_map/ppermute | solution.py:19
  47.8 22.1 %copy-start.2 = (f32[2048]{0:T(1024)S(1)}, f32[2048]{0:T(1024)}, u32[]{:S(2)}) copy-start(f32[2048]{0:T(1024)} %param.21) | copy-start | bytes 24580
  50.0 18.5 %all-to-all-start = ((bf16[4,64,2048]{2,1,0:T(8,128)(2,1)}), bf16[4,64,2048]{2,1,0:T(8,128)(2,1)S(1)}, u32[]{:S(2)}, u32[]{:S(2)}) async-start(bf16[4,64,2048]{2,1,0:T(8,128)(2,1)} %bitcast.23), calls=%async_computation | async-start | bytes 2097152 | tf_op jit(solution)/shard_map/all_to_all | solution.py:38
  86.8 6.0 %collective-permute-start.8 = (bf16[256,2048]{1,0:T(8,128)(2,1)S(1)}, bf16[256,2048]{1,0:T(8,128)(2,1)S(1)}, u32[]{:S(2)}, u32[]{:S(2)}) collective-permute-start(bf16[256,2048]{1,0:T(8,128)(2,1)S(1)} %bitcast.96), channel_id=1, source_target_pairs={{0,1},{1,0},{2,3},{3,2},{4,5},{5,4},{6,7},{7,6},{8,9},{9,8},{10,11... | collective-permute-start | bytes 3145736 | tf_op jit(solution)/shard_map/ppermute | solution.py:19
  121.6 8.8 %collective-permute-start.9 = (bf16[256,2048]{1,0:T(8,128)(2,1)}, bf16[256,2048]{1,0:T(8,128)(2,1)}, u32[]{:S(2)}, u32[]{:S(2)}) collective-permute-start(bf16[256,2048]{1,0:T(8,128)(2,1)} %fusion.16), channel_id=1, source_target_pairs={{0,1},{1,0},{2,3},{3,2},{4,5},{5,4},{6,7},{7,6},{8,9},{9,8},{10,11... | collective-permute-start | bytes 3145736 | tf_op jit(solution)/shard_map/ppermute | solution.py:19
  167.5 6.2 %collective-permute-start.10 = (bf16[256,2048]{1,0:T(8,128)(2,1)S(1)}, bf16[256,2048]{1,0:T(8,128)(2,1)S(1)}, u32[]{:S(2)}, u32[]{:S(2)}) collective-permute-start(bf16[256,2048]{1,0:T(8,128)(2,1)S(1)} %bitcast.94), channel_id=1, source_target_pairs={{0,1},{1,0},{2,3},{3,2},{4,5},{5,4},{6,7},{7,6},{8,9},{9,8},{10,11... | collective-permute-start | bytes 3145736 | tf_op jit(solution)/shard_map/ppermute | solution.py:19
Sparse Core Ops, SparseCore 0:
  10.4 104.4 all-gather.1
